TPU v7x, 32 devices: a whole 2x2x4 slice. The times are simulated.
32 devices in a mesh: grp: 2 (over x), tp: 16 (over z, y, core).
Axes of the slice: x: 2, y: 2, z: 4, core: 2. Of those that a mesh axis runs over, the one named last changes fastest.
Arguments:
- stream_in: bfloat16 [64, 4, 4096], P('grp'), parts along dimension 0, may hold values from -6 to 6
- state_in: float32 [2, 64, 8, 256, 256], P(None, 'grp', None, 'tp'), parts along dimension 1, may hold values from -0.8 to 0.8
- norm_gain: bfloat16 [2, 4096], replicated, may hold values from 0.099609375 to 1.8984375
- query_weight: bfloat16 [2, 4096, 2048], P(None, None, 'tp'), may hold values from -0.09375 to 0.09375
- key_weight: bfloat16 [2, 4096, 2048], P(None, None, 'tp'), may hold values from -0.09375 to 0.09375
- value_weight: bfloat16 [2, 4096, 8, 256], P(None, None, None, 'tp'), as said below
- gate_weight: bfloat16 [2, 4096, 8, 256], P(None, None, None, 'tp'), may hold values from -0.09375 to 0.09375
- group_gain: bfloat16 [2, 8, 256], P(None, None, 'tp'), may hold values from 0.099609375 to 1.8984375
- output_weight: bfloat16 [2, 8, 256, 4096], P(None, None, 'tp'), may hold values from -0.375 to 0.375
Outputs:
- stream_out: bfloat16 [64, 4, 4096], P('grp', None, 'tp'), parts along dimension 0
- state_out: float32 [2, 64, 8, 256, 256], P(None, 'grp', None, 'tp'), parts along dimension 1
There are 2 independent parts, one for each index of `grp`. A program takes and returns all parts, laid end to end along the dimension named above; an argument that names none is the same for every part. Nothing has to cross between parts.
Inputs may be any that keep to these rules, and one draw needn't show every extreme that they name: `value_weight`: real values; column scales of the value projection differ.
All inputs are finite; a program needn't handle non-finite values.
Results may differ from a plain program's by a relative error of at most 0.024.
Values may be sent and summed in bfloat16 or wider, within the bound.
A program may use at most 64 MiB of HBM per device.

v0:
```python
import jax
import jax.numpy as jnp
from jax import lax
from jax.sharding import PartitionSpec as P

HEAD_DIM = 256
PAST = 1024


EPS_RMS = 1e-06
EPS_GROUP = 1e-05
ROTARY_BASE = 10000.0


def log_decays(count):
    return jnp.log(1.0 - jnp.power(2.0, -5.0 - jnp.arange(count, dtype=jnp.float32)))


def decay_tables(log_gamma, count):
    steps = jnp.arange(count, dtype=jnp.float32)
    gap = steps[:, None] - steps[None, :]
    intra = jnp.where(
        gap[None] >= 0, jnp.exp(log_gamma[:, None, None] * jnp.maximum(gap, 0.0)[None]), 0.0
    )
    q_decay = jnp.exp(log_gamma[None, :] * (steps[:, None] + 1.0))
    k_decay = jnp.exp(log_gamma[None, :] * (count - 1.0 - steps[:, None]))
    block_decay = jnp.exp(log_gamma * count)
    return (intra, q_decay, k_decay, block_decay)


def rotate(values, offset):
    half_dim = values.shape[-1] // 2
    freqs = jnp.power(
        ROTARY_BASE, -jnp.arange(half_dim, dtype=jnp.float32) * (2.0 / values.shape[-1])
    )
    places = (offset + jnp.arange(values.shape[1])).astype(jnp.float32)
    angles = places[:, None] * freqs[None, :]
    cosine = jnp.cos(angles)[None, :, None, :]
    sine = jnp.sin(angles)[None, :, None, :]
    first = values[..., :half_dim]
    second = values[..., half_dim:]
    return jnp.concatenate(
        [first * cosine - second * sine, second * cosine + first * sine], axis=-1
    )


def local(
    stream_in,
    state_in,
    norm_gain,
    query_weight,
    key_weight,
    value_weight,
    gate_weight,
    group_gain,
    output_weight,
):
    seqs, new_tok, width = stream_in.shape
    heads, local_dim = (value_weight.shape[2], value_weight.shape[3])
    head_dim = HEAD_DIM
    log_gamma = log_decays(heads)
    intra, q_decay, k_decay, block_decay = decay_tables(log_gamma, new_tok)
    highest = lax.Precision.HIGHEST
    share_cols = width // lax.axis_size("tp")
    col_start = lax.axis_index("tp") * share_cols
    layers = state_in.shape[0]
    stream = stream_in
    stream_share = stream_in
    new_states = []
    for layer_no in range(layers):
        stream_f = stream.astype(jnp.float32)
        normed = stream_f * lax.rsqrt(
            jnp.mean(stream_f * stream_f, axis=-1, keepdims=True) + EPS_RMS
        )
        normed = (normed * norm_gain[layer_no].astype(jnp.float32)).astype(jnp.bfloat16)
        flat = normed.reshape(seqs * new_tok, width)
        query_part = jnp.dot(flat, query_weight[layer_no], preferred_element_type=jnp.float32)
        query_part = query_part.astype(jnp.bfloat16).reshape(seqs, new_tok, -1)
        key_part = jnp.dot(flat, key_weight[layer_no], preferred_element_type=jnp.float32)
        key_part = key_part.astype(jnp.bfloat16).reshape(seqs, new_tok, -1)

        def project_local(weight):
            result = jnp.dot(
                flat, weight.reshape(width, heads * local_dim), preferred_element_type=jnp.float32
            )
            result = lax.optimization_barrier(result.astype(jnp.bfloat16))
            return result.astype(jnp.float32).reshape(seqs, new_tok, heads, local_dim)

        values_f = project_local(value_weight[layer_no])
        gates_f = project_local(gate_weight[layer_no])
        queries, key_rows = (
            lax.all_gather(query_part, "tp", axis=2, tiled=True),
            lax.all_gather(key_part, "tp", axis=2, tiled=True),
        )
        queries = queries.astype(jnp.float32).reshape(seqs, new_tok, heads, head_dim)
        key_rows = key_rows.astype(jnp.float32).reshape(seqs, new_tok, heads, head_dim)
        rot_q = rotate(queries, PAST)
        rot_k = rotate(key_rows, PAST) * head_dim ** (-0.5)
        scores = jnp.einsum("bthd,bshd->bhts", rot_q, rot_k, precision=highest) * intra[None]
        inner = jnp.einsum("bhts,bshe->bthe", scores, values_f, precision=highest)
        state = state_in[layer_no]
        carried = (
            jnp.einsum("bthd,bhed->bthe", rot_q, state, precision=highest)
            * q_decay[None, :, :, None]
        )
        mixed = inner + carried
        new_state = state * block_decay[None, :, None, None] + jnp.einsum(
            "bthe,bthd->bhed", values_f, rot_k * k_decay[None, :, :, None], precision=highest
        )
        new_states.append(new_state)
        totals, squares = lax.psum((jnp.sum(mixed, axis=-1), jnp.sum(mixed * mixed, axis=-1)), "tp")
        mean_o = (totals / head_dim)[..., None]
        var_o = (squares / head_dim)[..., None] - mean_o * mean_o
        normal = (
            (mixed - mean_o)
            * lax.rsqrt(var_o + EPS_GROUP)
            * group_gain[layer_no].astype(jnp.float32)[None, None]
        )
        gated = (jax.nn.silu(gates_f) * normal).astype(jnp.bfloat16)
        partial_out = jnp.dot(
            gated.reshape(seqs * new_tok, heads * local_dim),
            output_weight[layer_no].reshape(heads * local_dim, width),
            preferred_element_type=jnp.float32,
        ).reshape(seqs, new_tok, width)
        share_out = lax.psum_scatter(partial_out, "tp", scatter_dimension=2, tiled=True)
        own_cols = lax.dynamic_slice_in_dim(stream, col_start, share_cols, 2)
        stream_share = (own_cols.astype(jnp.float32) + share_out).astype(jnp.bfloat16)
        if layer_no + 1 < layers:
            stream = lax.all_gather(stream_share, "tp", axis=2, tiled=True)
    result = stream_share
    return (result, jnp.stack(new_states))


def solution(mesh):
    in_specs = (
        P("grp", None, None),
        P(None, "grp", None, "tp", None),
        P(),
        P(None, None, "tp"),
        P(None, None, "tp"),
        P(None, None, None, "tp"),
        P(None, None, None, "tp"),
        P(None, None, "tp"),
        P(None, None, "tp", None),
    )
    out_specs = (P("grp", None, "tp"), P(None, "grp", None, "tp", None))
    return jax.shard_map(local, mesh=mesh, in_specs=in_specs, out_specs=out_specs, check_vma=False)
```

profile of v0, /device:TPU:0, one launch (start us, length us, event | category | flops | bytes accessed | tf_op | source)
XLA Modules:
  0.0 433.5 jit_solution(2907268632619906550)
XLA Ops:
  7.3 0.7 bitcast_convert_fusion
  8.0 1.8 fusion.10
  9.9 0.8 slice_convert_fusion
  10.7 1.9 fusion.12
  12.6 0.3 reshape.316
  12.9 1.8 convolution_convert_fusion.4
  14.8 0.4 convolution_convert_fusion.5
  15.2 24.6 %all_gather.15 = bf16[32,4,2048]{2,1,0:T(4,128)(2,1)S(1)} all-gather(bf16[32,4,128]{2,1,0:T(4,128)(2,1)S(1)} %bitcast.115), channel_id=1, replica_groups=mesh['grp'=2,'tp'=16] {'tp'}, dimensions={2}, use_global_device_ids=true | all-gather | bytes 557056 | tf_op jit(solution)/shard_map/all_gather | solution.py:92
  39.8 19.0 %all_gather.16 = bf16[32,4,2048]{2,1,0:T(4,128)(2,1)S(1)} all-gather(bf16[32,4,128]{2,1,0:T(4,128)(2,1)S(1)} %bitcast.114), channel_id=1, replica_groups=mesh['grp'=2,'tp'=16] {'tp'}, dimensions={2}, use_global_device_ids=true | all-gather | bytes 557056 | tf_op jit(solution)/shard_map/all_gather | solution.py:93
  58.9 0.1 convert.11
  59.0 0.1 convert.10
  59.3 0.6 multiply_subtract_fusion.2
  59.9 6.9 %fusion.4 = f32[32,8,4,16]{3,2,1,0:T(4,128)} fusion(f32[2,32,8,16,256]{4,3,2,1,0:T(8,128)} %param.10, f32[32,4,8,128]{3,1,2,0:T(4,128)S(1)} %get-tuple-element.46, f32[32,4,8,128]{3,1,2,0:T(4,128)S(1)} %get-tuple-element.47), kind=kOutput, calls=%fused_computation.7 | convolution fusion | flops 50593792 | bytes 5308416 | tf_op jit(solution)/shard_map/bthd,bhed->bthe/dot_general | solution.py:103
  66.8 2.0 copy.76
  68.9 2.7 fusion.56
  71.5 0.4 convolution_convert_fusion.6
  72.0 0.2 reshape.319
  72.3 2.3 convolution_multiply_fusion.1
  74.6 1.0 fusion.38
  75.6 0.3 copy.75
  75.9 2.7 fusion.55
  78.7 0.4 convolution_convert_fusion.7
  79.1 0.2 reshape.338
  79.3 0.3 copy.73
  79.6 1.8 fusion.54
  81.4 0.2 fusion.51
  81.6 59.1 %all-reduce.1 = (f32[32,4,8]{0,2,1:T(8,128)S(1)}, f32[32,4,8]{0,2,1:T(8,128)S(1)}) all-reduce(f32[32,4,8]{0,2,1:T(8,128)S(1)} %get-tuple-element.15, f32[32,4,8]{0,2,1:T(8,128)S(1)} %get-tuple-element.14), channel_id=1, replica_groups=mesh['grp'=2,'tp'=16] {'tp'}, use_global_device_ids=true, to_apply=%region_4.5 | all-reduce | flops 2048 | bytes 16384 | tf_op jit(solution)/shard_map/psum | solution.py:111
  140.9 1.8 fusion.57
  142.8 0.9 constant_dynamic-slice_fusion
  143.6 58.3 %reduce-scatter.3.cloned.1.call-done = f32[32,4,256]{2,0,1:T(8,128)} async-done(((f32[32,4,4096]{2,0,1:T(8,128)}), f32[32,4,256]{2,0,1:T(8,128)}) %reduce-scatter.3.cloned.1.call-update) | async-done | bytes 131088 | tf_op jit(solution)/shard_map/reduce_scatter | solution.py:125
  201.9 1.5 add_convert_fusion.1
  203.5 0.3 reduce-scatter.5.cloned.1.call-start
  203.8 36.5 %all-gather.2.cloned.1.call-done = bf16[32,4,4096]{2,0,1:T(8,128)(2,1)} async-done(((bf16[32,4,256]{2,0,1:T(8,128)(2,1)}), bf16[32,4,4096]{2,0,1:T(8,128)(2,1)}) %all-gather.2.cloned.1.call-update) | async-done | bytes 1048592 | tf_op jit(solution)/shard_map/all_gather | solution.py:129
  240.3 1.5 fusion.13
  241.8 1.5 fusion.15
  243.4 0.8 copy.78
  244.2 0.3 reshape.326
  244.5 1.7 convolution_convert_fusion
  246.2 1.7 convolution_convert_fusion.1
  248.0 0.4 convolution_convert_fusion.2
  248.4 0.4 convolution_convert_fusion.3
  248.9 0.2 reshape.329
  249.1 21.5 %all_gather.19 = bf16[32,4,2048]{2,1,0:T(4,128)(2,1)S(1)} all-gather(bf16[32,4,128]{2,1,0:T(4,128)(2,1)S(1)} %bitcast.113), channel_id=1, replica_groups=mesh['grp'=2,'tp'=16] {'tp'}, dimensions={2}, use_global_device_ids=true | all-gather | bytes 557056 | tf_op jit(solution)/shard_map/all_gather | solution.py:93
  270.6 18.9 %all_gather.18 = bf16[32,4,2048]{2,1,0:T(4,128)(2,1)S(1)} all-gather(bf16[32,4,128]{2,1,0:T(4,128)(2,1)S(1)} %bitcast.112), channel_id=1, replica_groups=mesh['grp'=2,'tp'=16] {'tp'}, dimensions={2}, use_global_device_ids=true | all-gather | bytes 557056 | tf_op jit(solution)/shard_map/all_gather | solution.py:92
  289.5 0.2 reshape.346
  289.6 1.0 copy.80
  290.7 0.1 convert.12
  290.8 0.1 convert.13
  291.0 0.5 multiply_subtract_fusion
  291.4 0.8 copy-done.8
  292.2 6.6 %fusion = f32[32,8,4,16]{3,2,1,0:T(4,128)} fusion(f32[2,32,8,16,256]{4,3,2,1,0:T(8,128)} %param.10, f32[32,4,8,128]{3,1,2,0:T(4,128)S(1)} %get-tuple-element.44, f32[32,4,8,128]{3,1,2,0:T(4,128)S(1)} %get-tuple-element.45), kind=kOutput, calls=%fused_computation.2 | convolution fusion | flops 50593792 | bytes 5308416 | tf_op jit(solution)/shard_map/bthd,bhed->bthe/dot_general | solution.py:103
  298.8 1.3 copy.83
  300.1 3.4 convolution_multiply_fusion
  303.5 1.0 fusion.35
  304.5 0.3 copy.82
  304.8 0.2 fusion.50
  305.0 59.2 %all-reduce = (f32[32,4,8]{0,2,1:T(8,128)S(1)}, f32[32,4,8]{0,2,1:T(8,128)S(1)}) all-reduce(f32[32,4,8]{0,2,1:T(8,128)S(1)} %get-tuple-element.13, f32[32,4,8]{0,2,1:T(8,128)S(1)} %get-tuple-element.12), channel_id=1, replica_groups=mesh['grp'=2,'tp'=16] {'tp'}, use_global_device_ids=true, to_apply=%region_10.11 | all-reduce | flops 2048 | bytes 16384 | tf_op jit(solution)/shard_map/psum | solution.py:111
  364.4 1.8 fusion.58
  366.3 4.5 %fusion.7 = f32[1,32,8,16,256]{4,3,2,1,0:T(8,128)S(1)} fusion(f32[2,32,8,16,256]{4,3,2,1,0:T(8,128)} %param.10, f32[8]{0:T(128)S(1)} %multiply_exponential_fusion.1, f32[32,4,8,128]{3,1,2,0:T(4,128)S(1)} %copy-done.5, f32[32,4,8,128]{3,1,2,0:T(4,128)S(1)} %copy-done.3, f32[4,8]{0,1:T(8,128)S(1)} %copy.85, bf16[32,4,8,16]{3,2,1,0:T(8,128)(2,1)S(1)} %reshape.319), kind=kOutput, calls=%fused_computation.10 | convolution fusion | flops 52953088 | bytes 9470112 | tf_op jit(solution)/shard_map/bthe,bthd->bhed/dot_general | solution.py:107
  370.8 4.5 %fusion.3 = f32[1,32,8,16,256]{4,3,2,1,0:T(8,128)S(1)} fusion(f32[2,32,8,16,256]{4,3,2,1,0:T(8,128)} %param.10, f32[8]{0:T(128)S(1)} %multiply_exponential_fusion.1, f32[32,4,8,128]{3,1,2,0:T(4,128)S(1)} %copy-done.7, f32[32,4,8,128]{3,1,2,0:T(4,128)S(1)} %get-tuple-element.28, f32[4,8]{0,1:T(8,128)S(1)} %copy.85, bf16[32,4,8,16]{3,2,1,0:T(8,128)(2,1)S(1)} %reshape.329), kind=kOutput, calls=%fused_computation.5 | convolution fusion | flops 52953088 | bytes 9470112 | tf_op jit(solution)/shard_map/bthe,bthd->bhed/dot_general | solution.py:107
  375.3 4.4 %pad_maximum_fusion = f32[2,32,8,16,256]{4,3,2,1,0:T(8,128)} fusion(f32[1,32,8,16,256]{4,3,2,1,0:T(8,128)S(1)} %fusion.3, f32[1,32,8,16,256]{4,3,2,1,0:T(8,128)S(1)} %fusion.7), kind=kLoop, calls=%fused_computation | loop fusion | flops 2097152 | bytes 16777216 | tf_op jit(solution)/shard_map/stack | solution.py:131
  379.8 45.6 %reduce-scatter.5.cloned.1.call-done = f32[32,4,256]{2,0,1:T(8,128)} async-done(((f32[32,4,4096]{2,0,1:T(8,128)}), f32[32,4,256]{2,0,1:T(8,128)}) %reduce-scatter.5.cloned.1.call-update) | async-done | bytes 131088 | tf_op jit(solution)/shard_map/reduce_scatter | solution.py:125
  425.4 0.9 add_convert_fusion
  426.3 0.7 copy.88
  (45 shorter events, 1.0 us)
Async XLA Ops:
  7.2 194.8 %reduce-scatter.3.cloned.1.call-start = ((), (), s32[]{:S(2)}) async-start(), calls=%async_computation.2 | async-start | bytes 2228224 | tf_op jit(solution)/shard_map/reduce_scatter | solution.py:125
  12.9 1.9 copy-start.11
  59.9 12.4 %copy-start.2 = (f32[32,4,8,128]{3,1,2,0:T(4,128)}, f32[32,4,8,128]{3,1,2,0:T(4,128)S(1)}, u32[]{:S(2)}) copy-start(f32[32,4,8,128]{3,1,2,0:T(4,128)S(1)} %get-tuple-element.32) | copy-start | bytes 1572868
  59.9 12.4 %copy-start.4 = (f32[32,4,8,128]{3,1,2,0:T(4,128)}, f32[32,4,8,128]{3,1,2,0:T(4,128)S(1)}, u32[]{:S(2)}) copy-start(f32[32,4,8,128]{3,1,2,0:T(4,128)S(1)} %get-tuple-element.33) | copy-start | bytes 1572868
  79.6 1.9 copy-start.9
  142.7 97.6 %all-gather.2.cloned.1.call-start = ((), (), s32[]{:S(2)}) async-start(), calls=%async_computation.3 | async-start | bytes 1114112 | tf_op jit(solution)/shard_map/all_gather | solution.py:129
  203.5 221.9 %reduce-scatter.5.cloned.1.call-start = ((), (), s32[]{:S(2)}) async-start(), calls=%async_computation.4 | async-start | bytes 2228224 | tf_op jit(solution)/shard_map/reduce_scatter | solution.py:125
  244.5 3.5 copy-start
  246.2 2.2 copy-start.1
  291.4 0.8 copy-start.8
  291.4 8.7 %copy-start.6 = (f32[32,4,8,128]{3,1,2,0:T(4,128)}, f32[32,4,8,128]{3,1,2,0:T(4,128)S(1)}, u32[]{:S(2)}) copy-start(f32[32,4,8,128]{3,1,2,0:T(4,128)S(1)} %get-tuple-element.29) | copy-start | bytes 1572868
  303.5 60.8 %copy-start.10 = (f32[32,4,8,16]{0,3,2,1:T(8,128)S(1)}, f32[32,4,8,16]{0,3,2,1:T(8,128)}, u32[]{:S(2)}) copy-start(f32[32,4,8,16]{0,3,2,1:T(8,128)} %copy.80) | copy-start | bytes 196612
  364.4 2.0 copy-start.3
  364.4 1.9 copy-start.5
  366.3 4.5 %copy-start.7 = (f32[32,4,8,128]{3,1,2,0:T(4,128)S(1)}, f32[32,4,8,128]{3,1,2,0:T(4,128)}, u32[]{:S(2)}) copy-start(f32[32,4,8,128]{3,1,2,0:T(4,128)} %copy-done.6) | copy-start | bytes 1572868
Sparse Core Ops, SparseCore 0:
  142.8 59.0 reduce-scatter.2
  204.7 35.5 all-gather.1
  366.3 58.9 reduce-scatter.4
where the time goes:
time: 434 us
  blocking collectives  202 us (47%)
  waiting for transfers between devices  140 us (32%)
  matrix products  41.1 us (9%)
  other arithmetic  17.9 us (4%)
  local copies, waits for them, and re-layouts  17.2 us (4%)
  between operations  14.2 us (3%)
    psum x2, blocking collectives, local(): lax.psum((jnp.sum(mixed, axis=-1), jnp.sum(mixed * mixed, axis=-1)), 'tp')  118 us
    reduce_scatter x2, waiting for transfers between devices, local(): lax.psum_scatter(partial_out, 'tp', scatter_dimension=2, tiled=True)  104 us
    all_gather x2, blocking collectives, local(): lax.all_gather(query_part, 'tp', axis=2, tiled=True)  43.5 us
    all_gather x2, blocking collectives, local(): lax.all_gather(key_part, 'tp', axis=2, tiled=True)  40.6 us
    all_gather x1, waiting for transfers between devices, local(): stream = lax.all_gather(stream_share, 'tp', axis=2, tiled=True)  36.5 us
    dot_general x2, matrix products, local(): jnp.einsum('bthd,bhed->bthe', rot_q, state, precision=highest)  13.5 us
    dot_general x2, matrix products, local(): jnp.einsum('bthe,bthd->bhed', values_f, rot_k * k_decay[None, :, :, None]...  8.98 us
  transfers between devices with their start and end apart: 3, of which 3 were waited for; matrix products, arithmetic and copies ran while one was open for 3% of the time, Pallas kernels for 0%

commit v1 on v0

--- a/solution.py
+++ b/solution.py
@@ -1,6 +1,11 @@
+import functools
+
 import jax
 import jax.numpy as jnp
+import numpy as np
 from jax import lax
+from jax.experimental import pallas as pl
+from jax.experimental.pallas import tpu as pltpu
 from jax.sharding import PartitionSpec as P
 
 HEAD_DIM = 256
@@ -44,7 +49,7 @@
     )
 
 
-def local(
+def plain_local(
     stream_in,
     state_in,
     norm_gain,
@@ -131,6 +136,360 @@
     return (result, jnp.stack(new_states))
 
 
+F32 = jnp.float32
+BF16 = jnp.bfloat16
+
+
+def nt_dot(a, b, precision=None):
+    return lax.dot_general(
+        a, b, (((1,), (1,)), ((), ())), preferred_element_type=F32, precision=precision
+    )
+
+
+def log2(value):
+    return int(value).bit_length() - 1
+
+
+def rotary_tables(heads, new_tok, head_dim):
+    half = head_dim // 2
+    freqs = np.power(
+        np.float32(ROTARY_BASE), -np.arange(half, dtype=np.float32) * np.float32(2.0 / head_dim)
+    ).astype(np.float32)
+    tok = np.arange(8) % new_tok
+    places = (PAST + tok).astype(np.float32)
+    angles = (places[:, None] * freqs[None, :]).astype(np.float32).astype(np.float64)
+    gamma = 1.0 - np.power(2.0, -5.0 - np.arange(heads))
+    grow = np.power(gamma[:, None], tok[None, :] + 1.0)[:, :, None]
+    shrink = head_dim ** (-0.5) / grow
+    cosine, sine = np.cos(angles)[None], np.sin(angles)[None]
+    block = np.broadcast_to(np.power(gamma, new_tok)[:, None, None], (heads, 8, half))
+    return np.stack(
+        [cosine * grow, sine * grow, cosine * shrink, sine * shrink, block]
+    ).astype(np.float32)
+
+
+def kernel(
+    n, head_dim,
+    x_hbm, st_hbm, ng_ref, qw_hbm, kw_hbm, vw_hbm, gw_hbm, gg_ref, ow_hbm, tab_ref,
+    y_ref, so_hbm,
+    xs, nv, wqk, wvg, wo, stv, qkg, kh, vts, sb, pbs, pbr, rss, rsr, mkc, mks, fold,
+    lsem, ag_s, ag_r, st_s, st_r, pb_s, pb_r, rs_s, rs_r, osem,
+):
+    layers, seqs, heads, e_dim, _ = st_hbm.shape
+    rows, width = x_hbm.shape
+    tok = rows // seqs
+    share = width // n
+    cols = qw_hbm.shape[2]
+    he = heads * e_dim
+    half = head_dim // 2
+    nc = n // 2
+    me = lax.axis_index("tp")
+    core = lax.rem(me, 2)
+    chip = lax.div(me, 2)
+    partner = chip * 2 + 1 - core
+
+    def away(o, c):
+        return lax.rem(chip + o, nc) * 2 + c
+
+    def back(o, c):
+        return lax.rem(chip - o + nc, nc) * 2 + c
+
+    def remote(src, dst, ssem, rsem, device):
+        return pltpu.make_async_remote_copy(
+            src_ref=src, dst_ref=dst, send_sem=ssem, recv_sem=rsem,
+            device_id={"tp": device}, device_id_type=pl.DeviceIdType.MESH,
+        )
+
+    loads = {}
+    count = 0
+
+    def load(name, src, dst):
+        nonlocal count
+        loads[name] = pltpu.make_async_copy(src, dst, lsem.at[count])
+        loads[name].start()
+        count += 1
+
+    for j in range(n):
+        load(("x", j), x_hbm.at[:, pl.ds(j * share, share)], xs.at[0, j])
+    for l in range(layers):
+        load(("q", l), qw_hbm.at[l], wqk.at[l, :, pl.ds(0, cols)])
+        load(("k", l), kw_hbm.at[l], wqk.at[l, :, pl.ds(cols, cols)])
+        load(("v", l), vw_hbm.at[l], wvg.at[l, pl.ds(0, he)])
+        load(("g", l), gw_hbm.at[l], wvg.at[l, pl.ds(he, he)])
+        load(("s", l), st_hbm.at[l], stv.at[l])
+        load(("o", l), ow_hbm.at[l], wo.at[l])
+
+    barrier = pltpu.get_barrier_semaphore()
+    for o in range(1, n):
+        pl.semaphore_signal(
+            barrier, inc=1, device_id={"tp": lax.rem(me + o, n)},
+            device_id_type=pl.DeviceIdType.MESH,
+        )
+
+    be = seqs * e_dim
+
+    def iota(shape, dim, shift=0):
+        return jnp.right_shift(lax.broadcasted_iota(jnp.int32, shape, dim), shift)
+
+    te, tt = log2(e_dim), log2(tok)
+    mkc[...] = (iota((rows, be), 0, tt) == iota((rows, be), 1, te)).astype(F32).astype(BF16)
+    mks[...] = (iota((be, rows), 0, te) == iota((be, rows), 1, tt)).astype(F32).astype(BF16)
+    low = e_dim - 1
+    fold[...] = (
+        jnp.bitwise_and(iota((be, he), 0), low) == jnp.bitwise_and(iota((be, he), 1), low)
+    ).astype(F32).astype(BF16)
+    causal = (
+        (iota((rows, rows), 0, tt) == iota((rows, rows), 1, tt))
+        & (iota((rows, rows), 0) >= iota((rows, rows), 1))
+    ).astype(F32)
+    heads_of = (iota((heads, he), 0) == iota((heads, he), 1, te)).astype(F32)
+    place = (
+        iota((e_dim, he), 0) == jnp.bitwise_and(iota((e_dim, he), 1), low)
+    ).astype(F32)
+    highest = lax.Precision.HIGHEST
+
+    def gather_start(buf, p):
+        sent = []
+        for o in range(1, nc):
+            sent.append(remote(buf.at[me], buf.at[me], ag_s.at[p, o], ag_r.at[p, o], away(o, core)))
+        sent.append(remote(buf.at[me], buf.at[me], ag_s.at[p, nc], ag_r.at[p, nc], partner))
+        for copy in sent:
+            copy.start()
+        return sent
+
+    def gather_finish(buf, p, sent):
+        for o in range(1, nc):
+            slot = buf.at[back(o, core)]
+            remote(slot, slot, ag_s.at[p, o], ag_r.at[p, o], partner).wait_recv()
+            copy = remote(slot, slot, ag_s.at[p, nc + o], ag_r.at[p, nc + o], partner)
+            copy.start()
+            sent.append(copy)
+        for o in range(nc):
+            slot = buf.at[back(o, 1 - core)]
+            remote(slot, slot, ag_s.at[p, nc + o], ag_r.at[p, nc + o], partner).wait_recv()
+
+    def spread(table):
+        return jnp.broadcast_to(table[None], (rows // 8, 8, half)).reshape(rows, half)
+
+    started = []
+    outs = []
+    for l in range(layers):
+        if l == 0:
+            for j in range(n):
+                loads[("x", j)].wait()
+
+        def square(j, acc):
+            block = xs[l, j].astype(F32)
+            return acc + block * block
+
+        total = lax.fori_loop(0, n, square, jnp.zeros((rows, share), F32))
+        scale = lax.rsqrt(jnp.sum(total, axis=1, keepdims=True) / width + EPS_RMS)
+
+        def normalise(j, carry):
+            at = pl.ds(pl.multiple_of(j * share, share), share)
+            gain = ng_ref[l : l + 1, at].astype(F32)
+            nv[:, at] = (xs[l, j].astype(F32) * scale * gain).astype(BF16)
+            return carry
+
+        lax.fori_loop(0, n, normalise, 0)
+        loads[("q", l)].wait()
+        loads[("k", l)].wait()
+        qkg[l, me] = jnp.dot(nv[...], wqk[l], preferred_element_type=F32).astype(BF16)
+        if l == 0:
+            pl.semaphore_wait(barrier, n - 1)
+        sent = gather_start(qkg.at[l], 2 * l)
+        loads[("v", l)].wait()
+        loads[("g", l)].wait()
+        vg = nt_dot(nv[...], wvg[l])
+        values = vg[:, :he].astype(BF16)
+        gates = vg[:, he:].astype(BF16).astype(F32)
+        vts[...] = jnp.transpose(values.astype(F32)).astype(BF16)
+        loads[("s", l)].wait()
+        gather_finish(qkg.at[l], 2 * l, sent)
+        started += sent
+
+        def mix(h, acc):
+            qk_a = qkg[l, 2 * h].astype(F32)
+            qk_b = qkg[l, 2 * h + 1].astype(F32)
+            qa, ka = qk_a[:, :half], qk_a[:, half:]
+            qb, kb = qk_b[:, :half], qk_b[:, half:]
+            cq, sq = spread(tab_ref[0, h]), spread(tab_ref[1, h])
+            ck, sk = spread(tab_ref[2, h]), spread(tab_ref[3, h])
+            rq = jnp.concatenate([qa * cq - qb * sq, qb * cq + qa * sq], axis=1).astype(BF16)
+            rk = jnp.concatenate([ka * ck - kb * sk, kb * ck + ka * sk], axis=1).astype(BF16)
+            kh[h] = rk
+            state = stv[l, :, h].reshape(be, head_dim).astype(BF16)
+            scores = (nt_dot(rq, rk) * causal).astype(BF16)
+            carried = nt_dot(rq, state).astype(BF16) * mkc[...]
+            part = jnp.dot(scores, values, preferred_element_type=F32)
+            part = part + jnp.dot(carried, fold[...], preferred_element_type=F32)
+            own = (iota((1, he), 1, te) == h).astype(F32)
+            return acc + part * own
+
+        mixed = lax.fori_loop(0, heads, mix, jnp.zeros((rows, he), F32))
+        sums = nt_dot(heads_of, mixed, highest)
+        squares = nt_dot(heads_of, mixed * mixed, highest)
+        sb[l, me] = jnp.concatenate([sums, squares], axis=0)
+        sent = []
+        for o in range(1, n):
+            sent.append(
+                remote(sb.at[l, me], sb.at[l, me], st_s.at[l, o], st_r.at[l, o], lax.rem(me + o, n))
+            )
+        for copy in sent:
+            copy.start()
+        started += sent
+
+        def update(h, carry):
+            at = pl.ds(pl.multiple_of(h * e_dim, e_dim), e_dim)
+            tall = jnp.broadcast_to(vts[at, :][None], (seqs, e_dim, rows)).reshape(be, rows)
+            fresh = jnp.dot(tall * mks[...], kh[h], preferred_element_type=F32)
+            row = tab_ref[4, h][0:1, :]
+            fade = jnp.concatenate([row, row], axis=1)
+            state = stv[l, :, h].reshape(be, head_dim)
+            stv[l, :, h] = ((state + fresh) * fade).reshape(seqs, e_dim, head_dim)
+            return carry
+
+        lax.fori_loop(0, heads, update, 0)
+
+        for o in range(1, n):
+            slot = sb.at[l, lax.rem(me - o + n, n)]
+            remote(slot, slot, st_s.at[l, o], st_r.at[l, o], partner).wait_recv()
+        out = pltpu.make_async_copy(stv.at[l], so_hbm.at[l], osem.at[l])
+        out.start()
+        outs.append(out)
+        stats = jnp.sum(sb[l], axis=0)
+        mean = stats[:heads] / head_dim
+        var = stats[heads:] / head_dim - mean * mean
+        rstd = lax.rsqrt(var + EPS_GROUP)
+
+        def expand(small):
+            return lax.dot_general(
+                small, heads_of, (((0,), (0,)), ((), ())),
+                preferred_element_type=F32, precision=highest,
+            )
+
+        gain = jnp.dot(gg_ref[l].astype(F32), place, preferred_element_type=F32, precision=highest)
+        gain = jnp.sum(gain * heads_of, axis=0, keepdims=True)
+        normal = (mixed - expand(mean)) * expand(rstd) * gain
+        gated = (gates / (1.0 + jnp.exp(-gates)) * normal).astype(BF16)
+
+        loads[("o", l)].wait()
+
+        def chunk(j):
+            at = pl.ds(pl.multiple_of(j * share, share), share)
+            return jnp.dot(gated, wo[l, :, at], preferred_element_type=F32)
+
+        order = list(range(1, nc)) + [0]
+        for o in order:
+            pbs[l, o] = chunk(away(o, 1 - core)).astype(BF16)
+            copy = remote(pbs.at[l, o], pbr.at[l, o], pb_s.at[l, o], pb_r.at[l, o], partner)
+            copy.start()
+            started.append(copy)
+        acc = None
+        for o in order:
+            own = chunk(away(o, core))
+            remote(pbs.at[l, o], pbr.at[l, o], pb_s.at[l, o], pb_r.at[l, o], partner).wait_recv()
+            own = own + pbr[l, o].astype(F32)
+            if o:
+                rss[l, o] = own.astype(BF16)
+                copy = remote(rss.at[l, o], rsr.at[l, o], rs_s.at[l, o], rs_r.at[l, o], away(o, core))
+                copy.start()
+                started.append(copy)
+            else:
+                acc = own
+        for o in range(1, nc):
+            remote(rss.at[l, o], rsr.at[l, o], rs_s.at[l, o], rs_r.at[l, o], partner).wait_recv()
+            acc = acc + rsr[l, o].astype(F32)
+        fresh_x = (xs[l, me].astype(F32) + acc).astype(BF16)
+        if l + 1 < layers:
+            xs[l + 1, me] = fresh_x
+            sent = gather_start(xs.at[l + 1], 2 * l + 1)
+            gather_finish(xs.at[l + 1], 2 * l + 1, sent)
+            started += sent
+        else:
+            y_ref[...] = fresh_x
+    for copy in started:
+        copy.wait_send()
+    for copy in outs:
+        copy.wait()
+
+
+def local(
+    stream_in, state_in, norm_gain, query_weight, key_weight,
+    value_weight, gate_weight, group_gain, output_weight,
+):
+    n = lax.axis_size("tp")
+    seqs, tok, width = stream_in.shape
+    layers, _, heads, e_dim, head_dim = state_in.shape
+    cols = query_weight.shape[2]
+    rows = seqs * tok
+    he = heads * e_dim
+    share = width // n
+    fits = (
+        cols == 128 and head_dim == 256 and he == 128 and heads == 8 and e_dim == 16
+        and share % 128 == 0 and n % 2 == 0 and rows == 128 and 8 % tok == 0
+    )
+    if not fits:
+        return plain_local(
+            stream_in, state_in, norm_gain, query_weight, key_weight,
+            value_weight, gate_weight, group_gain, output_weight,
+        )
+    nc = n // 2
+    be = seqs * e_dim
+    hbm = pl.BlockSpec(memory_space=pl.ANY)
+    vmem = pl.BlockSpec(memory_space=pltpu.VMEM)
+    dma = pltpu.SemaphoreType.DMA
+    tables = jnp.asarray(rotary_tables(heads, tok, head_dim))
+    flat = lambda w: jnp.transpose(w, (0, 2, 3, 1)).reshape(layers, he, width)
+    y, new_state = pl.pallas_call(
+        functools.partial(kernel, n, head_dim),
+        name="retention",
+        out_shape=(
+            jax.ShapeDtypeStruct((rows, share), BF16),
+            jax.ShapeDtypeStruct(state_in.shape, F32),
+        ),
+        in_specs=[hbm, hbm, vmem, hbm, hbm, hbm, hbm, vmem, hbm, vmem],
+        out_specs=(vmem, hbm),
+        scratch_shapes=[
+            pltpu.VMEM((layers, n, rows, share), BF16),
+            pltpu.VMEM((rows, width), BF16),
+            pltpu.VMEM((layers, width, 2 * cols), BF16),
+            pltpu.VMEM((layers, 2 * he, width), BF16),
+            pltpu.VMEM((layers, he, width), BF16),
+            pltpu.VMEM(state_in.shape, F32),
+            pltpu.VMEM((layers, n, rows, 2 * cols), BF16),
+            pltpu.VMEM((heads, rows, head_dim), BF16),
+            pltpu.VMEM((he, rows), BF16),
+            pltpu.VMEM((layers, n, 2 * heads, rows), F32),
+            pltpu.VMEM((layers, nc, rows, share), BF16),
+            pltpu.VMEM((layers, nc, rows, share), BF16),
+            pltpu.VMEM((layers, nc, rows, share), BF16),
+            pltpu.VMEM((layers, nc, rows, share), BF16),
+            pltpu.VMEM((rows, be), BF16),
+            pltpu.VMEM((be, rows), BF16),
+            pltpu.VMEM((be, he), BF16),
+            dma((n + 6 * layers,)),
+            dma((2 * layers, n)),
+            dma((2 * layers, n)),
+            dma((layers, n)),
+            dma((layers, n)),
+            dma((layers, nc)),
+            dma((layers, nc)),
+            dma((layers, nc)),
+            dma((layers, nc)),
+            dma((layers,)),
+        ],
+        compiler_params=pltpu.CompilerParams(
+            collective_id=0, has_side_effects=True, vmem_limit_bytes=60 * 2**20
+        ),
+    )(
+        stream_in.reshape(rows, width), state_in, norm_gain, query_weight, key_weight,
+        flat(value_weight), flat(gate_weight), group_gain,
+        output_weight.reshape(layers, he, width), tables,
+    )
+    return y.reshape(seqs, tok, share), new_state
+
+
 def solution(mesh):
     in_specs = (
         P("grp", None, None),

time: 434 us -> 110 us (0.25)
  blocking collectives: 202 us -> 0 us
  waiting for transfers between devices: 140 us -> 0 us
  Pallas kernels: 0 us -> 95.6 us
  matrix products: 41.1 us -> 0 us
  other arithmetic: 17.9 us -> 0 us
  between operations: 14.2 us -> 0.64 us
  local copies, waits for them, and re-layouts: 17.2 us -> 12.2 us
    psum x2 -> x0, blocking collectives: 118 us -> none  [local(): lax.psum((jnp.sum(mixed, axis=-1), jnp.sum(mixed * mixed, axis=-1)), 'tp')]
    reduce_scatter x2 -> x0, waiting for transfers between devices: 104 us -> none  [local(): lax.psum_scatter(partial_out, 'tp', scatter_dimension=2, tiled=True)]
    pallas_call x0 -> x1, Pallas kernels: none -> 95.6 us  [local(): pl.pallas_call(functools.partial(kernel, n, head_dim), name='retention',...]
    all_gather x4 -> x0, blocking collectives: 84 us -> none  [the longest x2 43.5 us: local(): lax.all_gather(query_part, 'tp', axis=2, tiled=True)]
    dot_general x18 -> x0, matrix products: 41.1 us -> none  [the longest x2 13.5 us: local(): jnp.einsum('bthd,bhed->bthe', rot_q, state, precision=highest)]
    all_gather x1 -> x0, waiting for transfers between devices: 36.5 us -> none  [local(): stream = lax.all_gather(stream_share, 'tp', axis=2, tiled=True)]
    convert_element_type x9 -> x0, other arithmetic: 7.69 us -> none  [the longest x2 3.43 us: local(): (normed * norm_gain[layer_no].astype(jnp.float32)).astype(jnp.bfloat16)]
    slice x3 -> x0, local copies, waits for them, and re-layouts: 7.17 us -> none  [the longest x1 2.74 us: local(): gates_f = project_local(gate_weight[layer_no])]
  transfers between devices with their start and end apart: 3 -> 0, of which waited for: 3 -> 0; matrix products, arithmetic and copies ran while one was open for 3% -> 0% of each run, Pallas kernels for 0% -> 0%
where the time goes in v1:
time: 110 us; the launch traced here: 108 us
  Pallas kernels  95.6 us (87%)
  local copies, waits for them, and re-layouts  12.2 us (11%)
    pallas_call x1, Pallas kernels, local(): pl.pallas_call(functools.partial(kernel, n, head_dim), name='retention',...  95.6 us
    unnamed x1, local copies, waits for them, and re-layouts  8.58 us

profile of v1, /device:TPU:0, one launch (start us, length us, event | category | flops | bytes accessed | tf_op | source)
XLA Modules:
  0.0 108.4 jit_solution(4647295022882905962)
XLA Ops:
  0.6 2.1 %reshape.19.x_hbm = bf16[128,4096]{1,0:T(8,128)(2,1)} reshape(bf16[32,4,4096]{2,1,0:T(4,128)(2,1)} %param.10) | data formatting | bytes 2097152 | tf_op jit(solution)/shard_map/reshape | solution.py:486
  2.8 95.6 %retention.1 = (bf16[128,256]{1,0:T(8,128)(2,1)}, f32[2,32,8,16,256]{4,3,2,1,0:T(8,128)}) custom-call(bf16[128,4096]{1,0:T(8,128)(2,1)} %reshape.19.x_hbm, f32[2,32,8,16,256]{4,3,2,1,0:T(8,128)} %st_hbm.1, bf16[2,4096]{1,0:T(2,128)(2,1)} %ng_ref.1, bf16[2,4096,128]{2,1,0:T(8,128)(2,1)} %qw_hbm.1, bf16[2,4096,128]{2,1,0:T(8,128)(2,1)} %kw_hbm.1, ...), custom_call_target="tpu_custom_call" | custom-call | tf_op jit(solution)/shard_map/retention/pallas_call | solution.py:444
  98.4 1.5 %reshape.23 = bf16[32,4,256]{2,1,0:T(4,128)(2,1)} reshape(bf16[128,256]{1,0:T(8,128)(2,1)} %get-tuple-element.4) | data formatting | bytes 131072 | tf_op jit(solution)/shard_map/reshape | solution.py:490
  99.9 8.6 %copy.13 = f32[2,32,8,16,256]{4,3,2,1,0:T(8,128)} copy(f32[2,32,8,16,256]{4,3,2,1,0:T(8,128)} %get-tuple-element.9) | data formatting | bytes 16777216

commit v2 on v1

--- a/solution.py
+++ b/solution.py
@@ -171,9 +171,9 @@
 def kernel(
     n, head_dim,
     x_hbm, st_hbm, ng_ref, qw_hbm, kw_hbm, vw_hbm, gw_hbm, gg_ref, ow_hbm, tab_ref,
-    y_ref, so_hbm,
-    xs, nv, wqk, wvg, wo, stv, qkg, kh, vts, sb, pbs, pbr, rss, rsr, mkc, mks, fold,
-    lsem, ag_s, ag_r, st_s, st_r, pb_s, pb_r, rs_s, rs_r, osem,
+    y_ref, stv,
+    xs, nv, wqk, wvg, wo, qkg, kh, vts, sb, pbs, pbr, yss, ysr, rss, rsr, mkc, mks, fold,
+    lsem, ag_s, ag_r, st_s, st_r, pb_s, pb_r, ys_s, ys_r, rs_s, rs_r,
 ):
     layers, seqs, heads, e_dim, _ = st_hbm.shape
     rows, width = x_hbm.shape
@@ -188,11 +188,14 @@
     chip = lax.div(me, 2)
     partner = chip * 2 + 1 - core
 
-    def away(o, c):
-        return lax.rem(chip + o, nc) * 2 + c
-
-    def back(o, c):
-        return lax.rem(chip - o + nc, nc) * 2 + c
+    nz = nc // 2
+    yy = lax.rem(chip, 2)
+    zz = lax.div(chip, 2)
+
+    def at_z(o, y, c):
+        return (lax.rem(zz + o + nz, nz) * 2 + y) * 2 + c
+
+    facing = at_z(0, 1 - yy, core)
 
     def remote(src, dst, ssem, rsem, device):
         return pltpu.make_async_remote_copy(
@@ -249,30 +252,42 @@
     highest = lax.Precision.HIGHEST
 
     def gather_start(buf, p):
-        sent = []
-        for o in range(1, nc):
-            sent.append(remote(buf.at[me], buf.at[me], ag_s.at[p, o], ag_r.at[p, o], away(o, core)))
-        sent.append(remote(buf.at[me], buf.at[me], ag_s.at[p, nc], ag_r.at[p, nc], partner))
+        own = buf.at[me]
+        sent = [remote(own, own, ag_s.at[p, nz], ag_r.at[p, nz], facing)]
+        for o in range(1, nz):
+            sent.append(remote(own, own, ag_s.at[p, o], ag_r.at[p, o], at_z(o, yy, core)))
+        sent.append(remote(own, own, ag_s.at[p, nc], ag_r.at[p, nc], partner))
         for copy in sent:
             copy.start()
         return sent
 
     def gather_finish(buf, p, sent):
-        for o in range(1, nc):
-            slot = buf.at[back(o, core)]
-            remote(slot, slot, ag_s.at[p, o], ag_r.at[p, o], partner).wait_recv()
-            copy = remote(slot, slot, ag_s.at[p, nc + o], ag_r.at[p, nc + o], partner)
+        def arrive(slot, k):
+            remote(slot, slot, ag_s.at[p, k], ag_r.at[p, k], partner).wait_recv()
+
+        def forward(slot, k, device):
+            copy = remote(slot, slot, ag_s.at[p, k], ag_r.at[p, k], device)
             copy.start()
             sent.append(copy)
-        for o in range(nc):
-            slot = buf.at[back(o, 1 - core)]
-            remote(slot, slot, ag_s.at[p, nc + o], ag_r.at[p, nc + o], partner).wait_recv()
+
+        for o in range(nz):
+            if o:
+                slot = buf.at[at_z(-o, yy, core)]
+                arrive(slot, o)
+                forward(slot, nz + o, facing)
+                forward(slot, nc + o, partner)
+        for o in range(nz):
+            slot = buf.at[at_z(-o, 1 - yy, core)]
+            arrive(slot, nz + o)
+            forward(slot, nc + nz + o, partner)
+        for o in range(nz):
+            arrive(buf.at[at_z(-o, yy, 1 - core)], nc + o)
+            arrive(buf.at[at_z(-o, 1 - yy, 1 - core)], nc + nz + o)
 
     def spread(table):
         return jnp.broadcast_to(table[None], (rows // 8, 8, half)).reshape(rows, half)
 
     started = []
-    outs = []
     for l in range(layers):
         if l == 0:
             for j in range(n):
@@ -354,9 +369,6 @@
         for o in range(1, n):
             slot = sb.at[l, lax.rem(me - o + n, n)]
             remote(slot, slot, st_s.at[l, o], st_r.at[l, o], partner).wait_recv()
-        out = pltpu.make_async_copy(stv.at[l], so_hbm.at[l], osem.at[l])
-        out.start()
-        outs.append(out)
         stats = jnp.sum(sb[l], axis=0)
         mean = stats[:heads] / head_dim
         var = stats[heads:] / head_dim - mean * mean
@@ -379,26 +391,43 @@
             at = pl.ds(pl.multiple_of(j * share, share), share)
             return jnp.dot(gated, wo[l, :, at], preferred_element_type=F32)
 
-        order = list(range(1, nc)) + [0]
+        order = list(range(1, nz)) + [0]
+        for side in (1, 0):
+            for o in order:
+                k = side * nz + o
+                y = 1 - yy if side else yy
+                pbs[l, k] = chunk(at_z(o, y, 1 - core)).astype(BF16)
+                copy = remote(pbs.at[l, k], pbr.at[l, k], pb_s.at[l, k], pb_r.at[l, k], partner)
+                copy.start()
+                started.append(copy)
+
+        def paired(o, side):
+            k = side * nz + o
+            own = chunk(at_z(o, 1 - yy if side else yy, core))
+            remote(pbs.at[l, k], pbr.at[l, k], pb_s.at[l, k], pb_r.at[l, k], partner).wait_recv()
+            return own + pbr[l, k].astype(F32)
+
         for o in order:
-            pbs[l, o] = chunk(away(o, 1 - core)).astype(BF16)
-            copy = remote(pbs.at[l, o], pbr.at[l, o], pb_s.at[l, o], pb_r.at[l, o], partner)
+            yss[l, o] = paired(o, 1).astype(BF16)
+            copy = remote(yss.at[l, o], ysr.at[l, o], ys_s.at[l, o], ys_r.at[l, o], facing)
             copy.start()
             started.append(copy)
         acc = None
         for o in order:
-            own = chunk(away(o, core))
-            remote(pbs.at[l, o], pbr.at[l, o], pb_s.at[l, o], pb_r.at[l, o], partner).wait_recv()
-            own = own + pbr[l, o].astype(F32)
+            own = paired(o, 0)
+            remote(yss.at[l, o], ysr.at[l, o], ys_s.at[l, o], ys_r.at[l, o], facing).wait_recv()
+            own = own + ysr[l, o].astype(F32)
             if o:
                 rss[l, o] = own.astype(BF16)
-                copy = remote(rss.at[l, o], rsr.at[l, o], rs_s.at[l, o], rs_r.at[l, o], away(o, core))
+                copy = remote(
+                    rss.at[l, o], rsr.at[l, o], rs_s.at[l, o], rs_r.at[l, o], at_z(o, yy, core)
+                )
                 copy.start()
                 started.append(copy)
             else:
                 acc = own
-        for o in range(1, nc):
-            remote(rss.at[l, o], rsr.at[l, o], rs_s.at[l, o], rs_r.at[l, o], partner).wait_recv()
+        for o in range(1, nz):
+            remote(rss.at[l, o], rsr.at[l, o], rs_s.at[l, o], rs_r.at[l, o], facing).wait_recv()
             acc = acc + rsr[l, o].astype(F32)
         fresh_x = (xs[l, me].astype(F32) + acc).astype(BF16)
         if l + 1 < layers:
@@ -410,7 +439,17 @@
             y_ref[...] = fresh_x
     for copy in started:
         copy.wait_send()
-    for copy in outs:
+
+
+def store_kernel(y_ref, state_ref, y_out, state_out, sem):
+    copies = [
+        pltpu.make_async_copy(state_ref.at[l], state_out.at[l], sem.at[l])
+        for l in range(state_ref.shape[0])
+    ]
+    for copy in copies:
+        copy.start()
+    y_out[...] = y_ref[...]
+    for copy in copies:
         copy.wait()
 
 
@@ -427,7 +466,7 @@
     share = width // n
     fits = (
         cols == 128 and head_dim == 256 and he == 128 and heads == 8 and e_dim == 16
-        and share % 128 == 0 and n % 2 == 0 and rows == 128 and 8 % tok == 0
+        and share % 128 == 0 and n % 4 == 0 and rows == 128 and 8 % tok == 0
     )
     if not fits:
         return plain_local(
@@ -446,25 +485,26 @@
         name="retention",
         out_shape=(
             jax.ShapeDtypeStruct((rows, share), BF16),
-            jax.ShapeDtypeStruct(state_in.shape, F32),
+            pltpu.VMEM(state_in.shape, F32),
         ),
         in_specs=[hbm, hbm, vmem, hbm, hbm, hbm, hbm, vmem, hbm, vmem],
-        out_specs=(vmem, hbm),
+        out_specs=(vmem, vmem),
         scratch_shapes=[
             pltpu.VMEM((layers, n, rows, share), BF16),
             pltpu.VMEM((rows, width), BF16),
             pltpu.VMEM((layers, width, 2 * cols), BF16),
             pltpu.VMEM((layers, 2 * he, width), BF16),
             pltpu.VMEM((layers, he, width), BF16),
-            pltpu.VMEM(state_in.shape, F32),
             pltpu.VMEM((layers, n, rows, 2 * cols), BF16),
             pltpu.VMEM((heads, rows, head_dim), BF16),
             pltpu.VMEM((he, rows), BF16),
             pltpu.VMEM((layers, n, 2 * heads, rows), F32),
             pltpu.VMEM((layers, nc, rows, share), BF16),
             pltpu.VMEM((layers, nc, rows, share), BF16),
-            pltpu.VMEM((layers, nc, rows, share), BF16),
-            pltpu.VMEM((layers, nc, rows, share), BF16),
+            pltpu.VMEM((layers, nc // 2, rows, share), BF16),
+            pltpu.VMEM((layers, nc // 2, rows, share), BF16),
+            pltpu.VMEM((layers, nc // 2, rows, share), BF16),
+            pltpu.VMEM((layers, nc // 2, rows, share), BF16),
             pltpu.VMEM((rows, be), BF16),
             pltpu.VMEM((be, rows), BF16),
             pltpu.VMEM((be, he), BF16),
@@ -475,18 +515,31 @@
             dma((layers, n)),
             dma((layers, nc)),
             dma((layers, nc)),
-            dma((layers, nc)),
-            dma((layers, nc)),
-            dma((layers,)),
+            dma((layers, nc // 2)),
+            dma((layers, nc // 2)),
+            dma((layers, nc // 2)),
+            dma((layers, nc // 2)),
         ],
         compiler_params=pltpu.CompilerParams(
-            collective_id=0, has_side_effects=True, vmem_limit_bytes=60 * 2**20
+            collective_id=0, has_side_effects=True, vmem_limit_bytes=44 * 2**20
         ),
     )(
         stream_in.reshape(rows, width), state_in, norm_gain, query_weight, key_weight,
         flat(value_weight), flat(gate_weight), group_gain,
         output_weight.reshape(layers, he, width), tables,
     )
+    y, new_state = pl.pallas_call(
+        store_kernel,
+        name="store",
+        out_shape=(
+            jax.ShapeDtypeStruct((rows, share), BF16),
+            jax.ShapeDtypeStruct(state_in.shape, F32),
+        ),
+        in_specs=[vmem, hbm],
+        out_specs=(vmem, hbm),
+        scratch_shapes=[dma((layers,))],
+        compiler_params=pltpu.CompilerParams(vmem_limit_bytes=2 * 2**20),
+    )(y, new_state)
     return y.reshape(seqs, tok, share), new_state
 
 

time: 110 us -> 95.3 us (0.87); the launches traced: 108 us -> 95.1 us
  local copies, waits for them, and re-layouts: 12.2 us -> 2.06 us
  Pallas kernels: 95.6 us -> 92.4 us
    unnamed x1 -> x6, local copies, waits for them, and re-layouts: 8.58 us -> 0.02 us
    pallas_call x1, Pallas kernels: 95.6 us -> 88.9 us  [local(): pl.pallas_call(functools.partial(kernel, n, head_dim), name='retention',...]
    pallas_call x0 -> x1, Pallas kernels: none -> 3.41 us  [local(): pl.pallas_call(store_kernel, name='store', out_shape=(jax.ShapeDtypeStruc...]
where the time goes in v2:
time: 95.3 us; the launch traced here: 95.1 us
  Pallas kernels  92.4 us (97%)
  local copies, waits for them, and re-layouts  2.06 us (2%)
    pallas_call x1, Pallas kernels, local(): pl.pallas_call(functools.partial(kernel, n, head_dim), name='retention',...  88.9 us
    pallas_call x1, Pallas kernels, local(): pl.pallas_call(store_kernel, name='store', out_shape=(jax.ShapeDtypeStruc...  3.41 us

profile of v2, /device:TPU:0, one launch (start us, length us, event | category | flops | bytes accessed | tf_op | source)
XLA Modules:
  0.0 95.1 jit_solution(7732221900384415268)
XLA Ops:
  0.6 0.0 copy-start
  0.6 0.0 copy-start.2
  0.7 0.0 copy-start.1
  0.7 1.4 %reshape.19.x_hbm = bf16[128,4096]{1,0:T(8,128)(2,1)S(1)} reshape(bf16[32,4,4096]{2,1,0:T(4,128)(2,1)} %param.10) | data formatting | bytes 2097152 | tf_op jit(solution)/shard_map/reshape | solution.py:527
  2.1 0.0 copy-done
  2.1 0.0 copy-done.2
  2.1 0.0 copy-done.1
  2.1 88.9 %retention.1 = (bf16[128,256]{1,0:T(8,128)(2,1)S(1)}, f32[2,32,8,16,256]{4,3,2,1,0:T(8,128)S(1)}) custom-call(bf16[128,4096]{1,0:T(8,128)(2,1)S(1)} %reshape.19.x_hbm, f32[2,32,8,16,256]{4,3,2,1,0:T(8,128)} %st_hbm.1, bf16[2,4096]{1,0:T(2,128)(2,1)S(1)} %copy-done.1, bf16[2,4096,128]{2,1,0:T(8,128)(2,1)} %qw_hbm.1, bf16[2,4096,128]{2,1,0:T(8,128)(2,1)} %kw_hbm.1, ...), custom_call_target="tpu_custom_call" | custom-call | tf_op jit(solution)/shard_map/retention/pallas_call | solution.py:483
  91.0 3.4 %store.1 = (bf16[128,256]{1,0:T(8,128)(2,1)S(1)}, f32[2,32,8,16,256]{4,3,2,1,0:T(8,128)}) custom-call(bf16[128,256]{1,0:T(8,128)(2,1)S(1)} %get-tuple-element.6.y_ref, f32[2,32,8,16,256]{4,3,2,1,0:T(8,128)S(1)} %get-tuple-element.7.state_ref), custom_call_target="tpu_custom_call" | custom-call | tf_op jit(solution)/shard_map/store/pallas_call | solution.py:531
  94.5 0.7 reshape.23
Async XLA Ops:
  0.6 1.4 %copy-start = (f32[5,8,8,128]{3,2,1,0:T(8,128)S(1)}, f32[5,8,8,128]{3,2,1,0:T(8,128)}, u32[]{:S(2)}) copy-start(f32[5,8,8,128]{3,2,1,0:T(8,128)} %constant.2.clone.tab_ref) | copy-start | bytes 491524
  0.6 1.4 %copy-start.2 = (bf16[2,8,16]{2,1,0:T(8,128)(2,1)S(1)}, bf16[2,8,16]{2,1,0:T(8,128)(2,1)}, u32[]{:S(2)}) copy-start(bf16[2,8,16]{2,1,0:T(8,128)(2,1)} %gg_ref.1) | copy-start | bytes 1540
  0.7 1.4 %copy-start.1 = (bf16[2,4096]{1,0:T(2,128)(2,1)S(1)}, bf16[2,4096]{1,0:T(2,128)(2,1)}, u32[]{:S(2)}) copy-start(bf16[2,4096]{1,0:T(2,128)(2,1)} %ng_ref.1) | copy-start | bytes 49156

commit v3 on v2

--- a/solution.py
+++ b/solution.py
@@ -136,6 +136,7 @@
     return (result, jnp.stack(new_states))
 
 
+LAG = 0
 F32 = jnp.float32
 BF16 = jnp.bfloat16
 
@@ -169,15 +170,17 @@
 
 
 def kernel(
-    n, head_dim,
+    n, head_dim, groups, lag,
     x_hbm, st_hbm, ng_ref, qw_hbm, kw_hbm, vw_hbm, gw_hbm, gg_ref, ow_hbm, tab_ref,
     y_ref, stv,
     xs, nv, wqk, wvg, wo, qkg, kh, vts, sb, pbs, pbr, yss, ysr, rss, rsr, mkc, mks, fold,
     lsem, ag_s, ag_r, st_s, st_r, pb_s, pb_r, ys_s, ys_r, rs_s, rs_r,
 ):
     layers, seqs, heads, e_dim, _ = st_hbm.shape
-    rows, width = x_hbm.shape
-    tok = rows // seqs
+    tok = x_hbm.shape[0] // seqs
+    width = x_hbm.shape[1]
+    seqs = seqs // groups
+    rows = seqs * tok
     share = width // n
     cols = qw_hbm.shape[2]
     he = heads * e_dim
@@ -193,9 +196,15 @@
     zz = lax.div(chip, 2)
 
     def at_z(o, y, c):
-        return (lax.rem(zz + o + nz, nz) * 2 + y) * 2 + c
+        z, bit = zz, 1
+        while bit < nz:
+            if o & bit:
+                z = z + bit - 2 * bit * lax.rem(lax.div(z, bit), 2)
+            bit = 2 * bit
+        return (z * 2 + y) * 2 + c
 
     facing = at_z(0, 1 - yy, core)
+    far = list(range(2, nz)) + [1]
 
     def remote(src, dst, ssem, rsem, device):
         return pltpu.make_async_remote_copy(
@@ -212,8 +221,10 @@
         loads[name].start()
         count += 1
 
-    for j in range(n):
-        load(("x", j), x_hbm.at[:, pl.ds(j * share, share)], xs.at[0, j])
+    for g in range(groups):
+        for j in range(n):
+            source = x_hbm.at[pl.ds(g * rows, rows), pl.ds(j * share, share)]
+            load(("x", g, j), source, xs.at[g, j])
     for l in range(layers):
         load(("q", l), qw_hbm.at[l], wqk.at[l, :, pl.ds(0, cols)])
         load(("k", l), kw_hbm.at[l], wqk.at[l, :, pl.ds(cols, cols)])
@@ -254,7 +265,7 @@
     def gather_start(buf, p):
         own = buf.at[me]
         sent = [remote(own, own, ag_s.at[p, nz], ag_r.at[p, nz], facing)]
-        for o in range(1, nz):
+        for o in far:
             sent.append(remote(own, own, ag_s.at[p, o], ag_r.at[p, o], at_z(o, yy, core)))
         sent.append(remote(own, own, ag_s.at[p, nc], ag_r.at[p, nc], partner))
         for copy in sent:
@@ -270,173 +281,200 @@
             copy.start()
             sent.append(copy)
 
+        for o in range(1, nz):
+            slot = buf.at[at_z(o, yy, core)]
+            arrive(slot, o)
+            forward(slot, nz + o, facing)
+            forward(slot, nc + o, partner)
+        yield
         for o in range(nz):
-            if o:
-                slot = buf.at[at_z(-o, yy, core)]
-                arrive(slot, o)
-                forward(slot, nz + o, facing)
-                forward(slot, nc + o, partner)
-        for o in range(nz):
-            slot = buf.at[at_z(-o, 1 - yy, core)]
+            slot = buf.at[at_z(o, 1 - yy, core)]
             arrive(slot, nz + o)
             forward(slot, nc + nz + o, partner)
+        yield
         for o in range(nz):
-            arrive(buf.at[at_z(-o, yy, 1 - core)], nc + o)
-            arrive(buf.at[at_z(-o, 1 - yy, 1 - core)], nc + nz + o)
+            arrive(buf.at[at_z(o, yy, 1 - core)], nc + o)
+            arrive(buf.at[at_z(o, 1 - yy, 1 - core)], nc + nz + o)
 
     def spread(table):
         return jnp.broadcast_to(table[None], (rows // 8, 8, half)).reshape(rows, half)
 
     started = []
-    for l in range(layers):
-        if l == 0:
-            for j in range(n):
-                loads[("x", j)].wait()
-
-        def square(j, acc):
-            block = xs[l, j].astype(F32)
-            return acc + block * block
-
-        total = lax.fori_loop(0, n, square, jnp.zeros((rows, share), F32))
-        scale = lax.rsqrt(jnp.sum(total, axis=1, keepdims=True) / width + EPS_RMS)
-
-        def normalise(j, carry):
-            at = pl.ds(pl.multiple_of(j * share, share), share)
-            gain = ng_ref[l : l + 1, at].astype(F32)
-            nv[:, at] = (xs[l, j].astype(F32) * scale * gain).astype(BF16)
-            return carry
-
-        lax.fori_loop(0, n, normalise, 0)
-        loads[("q", l)].wait()
-        loads[("k", l)].wait()
-        qkg[l, me] = jnp.dot(nv[...], wqk[l], preferred_element_type=F32).astype(BF16)
-        if l == 0:
-            pl.semaphore_wait(barrier, n - 1)
-        sent = gather_start(qkg.at[l], 2 * l)
-        loads[("v", l)].wait()
-        loads[("g", l)].wait()
-        vg = nt_dot(nv[...], wvg[l])
-        values = vg[:, :he].astype(BF16)
-        gates = vg[:, he:].astype(BF16).astype(F32)
-        vts[...] = jnp.transpose(values.astype(F32)).astype(BF16)
-        loads[("s", l)].wait()
-        gather_finish(qkg.at[l], 2 * l, sent)
-        started += sent
-
-        def mix(h, acc):
-            qk_a = qkg[l, 2 * h].astype(F32)
-            qk_b = qkg[l, 2 * h + 1].astype(F32)
-            qa, ka = qk_a[:, :half], qk_a[:, half:]
-            qb, kb = qk_b[:, :half], qk_b[:, half:]
-            cq, sq = spread(tab_ref[0, h]), spread(tab_ref[1, h])
-            ck, sk = spread(tab_ref[2, h]), spread(tab_ref[3, h])
-            rq = jnp.concatenate([qa * cq - qb * sq, qb * cq + qa * sq], axis=1).astype(BF16)
-            rk = jnp.concatenate([ka * ck - kb * sk, kb * ck + ka * sk], axis=1).astype(BF16)
-            kh[h] = rk
-            state = stv[l, :, h].reshape(be, head_dim).astype(BF16)
-            scores = (nt_dot(rq, rk) * causal).astype(BF16)
-            carried = nt_dot(rq, state).astype(BF16) * mkc[...]
-            part = jnp.dot(scores, values, preferred_element_type=F32)
-            part = part + jnp.dot(carried, fold[...], preferred_element_type=F32)
-            own = (iota((1, he), 1, te) == h).astype(F32)
-            return acc + part * own
-
-        mixed = lax.fori_loop(0, heads, mix, jnp.zeros((rows, he), F32))
-        sums = nt_dot(heads_of, mixed, highest)
-        squares = nt_dot(heads_of, mixed * mixed, highest)
-        sb[l, me] = jnp.concatenate([sums, squares], axis=0)
-        sent = []
-        for o in range(1, n):
-            sent.append(
-                remote(sb.at[l, me], sb.at[l, me], st_s.at[l, o], st_r.at[l, o], lax.rem(me + o, n))
-            )
-        for copy in sent:
-            copy.start()
-        started += sent
-
-        def update(h, carry):
-            at = pl.ds(pl.multiple_of(h * e_dim, e_dim), e_dim)
-            tall = jnp.broadcast_to(vts[at, :][None], (seqs, e_dim, rows)).reshape(be, rows)
-            fresh = jnp.dot(tall * mks[...], kh[h], preferred_element_type=F32)
-            row = tab_ref[4, h][0:1, :]
-            fade = jnp.concatenate([row, row], axis=1)
-            state = stv[l, :, h].reshape(be, head_dim)
-            stv[l, :, h] = ((state + fresh) * fade).reshape(seqs, e_dim, head_dim)
-            return carry
-
-        lax.fori_loop(0, heads, update, 0)
-
-        for o in range(1, n):
-            slot = sb.at[l, lax.rem(me - o + n, n)]
-            remote(slot, slot, st_s.at[l, o], st_r.at[l, o], partner).wait_recv()
-        stats = jnp.sum(sb[l], axis=0)
-        mean = stats[:heads] / head_dim
-        var = stats[heads:] / head_dim - mean * mean
-        rstd = lax.rsqrt(var + EPS_GROUP)
-
-        def expand(small):
-            return lax.dot_general(
-                small, heads_of, (((0,), (0,)), ((), ())),
-                preferred_element_type=F32, precision=highest,
-            )
-
-        gain = jnp.dot(gg_ref[l].astype(F32), place, preferred_element_type=F32, precision=highest)
-        gain = jnp.sum(gain * heads_of, axis=0, keepdims=True)
-        normal = (mixed - expand(mean)) * expand(rstd) * gain
-        gated = (gates / (1.0 + jnp.exp(-gates)) * normal).astype(BF16)
-
-        loads[("o", l)].wait()
-
-        def chunk(j):
-            at = pl.ds(pl.multiple_of(j * share, share), share)
-            return jnp.dot(gated, wo[l, :, at], preferred_element_type=F32)
-
-        order = list(range(1, nz)) + [0]
-        for side in (1, 0):
+    waited = set()
+
+    def once(key):
+        if key not in waited:
+            waited.add(key)
+            loads[key].wait()
+
+    def chain(g):
+        mine = pl.ds(g * seqs, seqs)
+        for l in range(layers):
+            lg = l * groups + g
+            if l == 0:
+                for j in range(n):
+                    loads[("x", g, j)].wait()
+
+            def square(j, acc):
+                block = xs[lg, j].astype(F32)
+                return acc + block * block
+
+            total = lax.fori_loop(0, n, square, jnp.zeros((rows, share), F32))
+            scale = lax.rsqrt(jnp.sum(total, axis=1, keepdims=True) / width + EPS_RMS)
+
+            def normalise(j, carry):
+                at = pl.ds(pl.multiple_of(j * share, share), share)
+                gain = ng_ref[l : l + 1, at].astype(F32)
+                nv[g, :, at] = (xs[lg, j].astype(F32) * scale * gain).astype(BF16)
+                return carry
+
+            lax.fori_loop(0, n, normalise, 0)
+            once(("q", l))
+            once(("k", l))
+            qkg[lg, me] = jnp.dot(nv[g], wqk[l], preferred_element_type=F32).astype(BF16)
+            if l == 0 and g == 0:
+                pl.semaphore_wait(barrier, n - 1)
+            sent = gather_start(qkg.at[lg], lg)
+            once(("v", l))
+            once(("g", l))
+            vg = nt_dot(nv[g], wvg[l])
+            values = vg[:, :he].astype(BF16)
+            gates = vg[:, he:].astype(BF16).astype(F32)
+            vts[g] = jnp.transpose(values.astype(F32)).astype(BF16)
+            once(("s", l))
+            yield
+            yield from gather_finish(qkg.at[lg], lg, sent)
+            started.extend(sent)
+
+            def mix(h, acc):
+                qk_a = qkg[lg, 2 * h].astype(F32)
+                qk_b = qkg[lg, 2 * h + 1].astype(F32)
+                qa, ka = qk_a[:, :half], qk_a[:, half:]
+                qb, kb = qk_b[:, :half], qk_b[:, half:]
+                cq, sq = spread(tab_ref[0, h]), spread(tab_ref[1, h])
+                ck, sk = spread(tab_ref[2, h]), spread(tab_ref[3, h])
+                rq = jnp.concatenate([qa * cq - qb * sq, qb * cq + qa * sq], axis=1).astype(BF16)
+                rk = jnp.concatenate([ka * ck - kb * sk, kb * ck + ka * sk], axis=1).astype(BF16)
+                kh[g * heads + h] = rk
+                state = stv[l, mine, h].reshape(be, head_dim).astype(BF16)
+                scores = (nt_dot(rq, rk) * causal).astype(BF16)
+                carried = nt_dot(rq, state).astype(BF16) * mkc[...]
+                part = jnp.dot(scores, values, preferred_element_type=F32)
+                part = part + jnp.dot(carried, fold[...], preferred_element_type=F32)
+                own = (iota((1, he), 1, te) == h).astype(F32)
+                return acc + part * own
+
+            mixed = lax.fori_loop(0, heads, mix, jnp.zeros((rows, he), F32), unroll=True)
+            sums = nt_dot(heads_of, mixed, highest)
+            squares = nt_dot(heads_of, mixed * mixed, highest)
+            sb[lg, me] = jnp.concatenate([sums, squares], axis=1)
+            sent = []
+            for o in range(1, n):
+                sent.append(
+                    remote(sb.at[lg, me], sb.at[lg, me], st_s.at[lg, o], st_r.at[lg, o], lax.rem(me + o, n))
+                )
+            for copy in sent:
+                copy.start()
+            started.extend(sent)
+
+            def update(h, carry):
+                at = pl.ds(pl.multiple_of(h * e_dim, e_dim), e_dim)
+                tall = jnp.broadcast_to(vts[g, at, :][None], (seqs, e_dim, rows)).reshape(be, rows)
+                fresh = jnp.dot(tall * mks[...], kh[g * heads + h], preferred_element_type=F32)
+                row = tab_ref[4, h][0:1, :]
+                fade = jnp.concatenate([row, row], axis=1)
+                state = stv[l, mine, h].reshape(be, head_dim)
+                stv[l, mine, h] = ((state + fresh) * fade).reshape(seqs, e_dim, head_dim)
+                return carry
+
+            lax.fori_loop(0, heads, update, 0, unroll=True)
+            yield
+
+            for o in range(1, n):
+                slot = sb.at[lg, lax.rem(me - o + n, n)]
+                remote(slot, slot, st_s.at[lg, o], st_r.at[lg, o], partner).wait_recv()
+            stats = jnp.sum(sb[lg], axis=0)
+            mean = stats[:, :rows] / head_dim
+            var = stats[:, rows:] / head_dim - mean * mean
+            rstd = lax.rsqrt(var + EPS_GROUP)
+
+            def expand(small):
+                return lax.dot_general(
+                    small, heads_of, (((0,), (0,)), ((), ())),
+                    preferred_element_type=F32, precision=highest,
+                )
+
+            gain = jnp.dot(gg_ref[l].astype(F32), place, preferred_element_type=F32, precision=highest)
+            gain = jnp.sum(gain * heads_of, axis=0, keepdims=True)
+            normal = (mixed - expand(mean)) * expand(rstd) * gain
+            gated = (gates / (1.0 + jnp.exp(-gates)) * normal).astype(BF16)
+
+            once(("o", l))
+
+            def chunk(j):
+                at = pl.ds(pl.multiple_of(j * share, share), share)
+                return jnp.dot(gated, wo[l, :, at], preferred_element_type=F32)
+
+            order = far + [0]
+            for side in (1, 0):
+                for o in order:
+                    k = side * nz + o
+                    y = 1 - yy if side else yy
+                    pbs[lg, k] = chunk(at_z(o, y, 1 - core)).astype(BF16)
+                    copy = remote(pbs.at[lg, k], pbr.at[lg, k], pb_s.at[lg, k], pb_r.at[lg, k], partner)
+                    copy.start()
+                    started.append(copy)
+
+            yield
+
+            def paired(o, side):
+                k = side * nz + o
+                own = chunk(at_z(o, 1 - yy if side else yy, core))
+                remote(pbs.at[lg, k], pbr.at[lg, k], pb_s.at[lg, k], pb_r.at[lg, k], partner).wait_recv()
+                return own + pbr[lg, k].astype(F32)
+
             for o in order:
-                k = side * nz + o
-                y = 1 - yy if side else yy
-                pbs[l, k] = chunk(at_z(o, y, 1 - core)).astype(BF16)
-                copy = remote(pbs.at[l, k], pbr.at[l, k], pb_s.at[l, k], pb_r.at[l, k], partner)
+                yss[lg, o] = paired(o, 1).astype(BF16)
+                copy = remote(yss.at[lg, o], ysr.at[lg, o], ys_s.at[lg, o], ys_r.at[lg, o], facing)
                 copy.start()
                 started.append(copy)
-
-        def paired(o, side):
-            k = side * nz + o
-            own = chunk(at_z(o, 1 - yy if side else yy, core))
-            remote(pbs.at[l, k], pbr.at[l, k], pb_s.at[l, k], pb_r.at[l, k], partner).wait_recv()
-            return own + pbr[l, k].astype(F32)
-
-        for o in order:
-            yss[l, o] = paired(o, 1).astype(BF16)
-            copy = remote(yss.at[l, o], ysr.at[l, o], ys_s.at[l, o], ys_r.at[l, o], facing)
-            copy.start()
-            started.append(copy)
-        acc = None
-        for o in order:
-            own = paired(o, 0)
-            remote(yss.at[l, o], ysr.at[l, o], ys_s.at[l, o], ys_r.at[l, o], facing).wait_recv()
-            own = own + ysr[l, o].astype(F32)
-            if o:
-                rss[l, o] = own.astype(BF16)
-                copy = remote(
-                    rss.at[l, o], rsr.at[l, o], rs_s.at[l, o], rs_r.at[l, o], at_z(o, yy, core)
-                )
-                copy.start()
-                started.append(copy)
+            yield
+            acc = None
+            for o in order:
+                own = paired(o, 0)
+                remote(yss.at[lg, o], ysr.at[lg, o], ys_s.at[lg, o], ys_r.at[lg, o], facing).wait_recv()
+                own = own + ysr[lg, o].astype(F32)
+                if o:
+                    rss[lg, o] = own.astype(BF16)
+                    copy = remote(
+                        rss.at[lg, o], rsr.at[lg, o], rs_s.at[lg, o], rs_r.at[lg, o], at_z(o, yy, core)
+                    )
+                    copy.start()
+                    started.append(copy)
+                else:
+                    acc = own
+            yield
+            for o in range(1, nz):
+                remote(rss.at[lg, o], rsr.at[lg, o], rs_s.at[lg, o], rs_r.at[lg, o], facing).wait_recv()
+                acc = acc + rsr[lg, o].astype(F32)
+            fresh_x = (xs[lg, me].astype(F32) + acc).astype(BF16)
+            if l + 1 < layers:
+                xs[lg + groups, me] = fresh_x
+                sent = gather_start(xs.at[lg + groups], layers * groups + lg)
+                yield
+                yield from gather_finish(xs.at[lg + groups], layers * groups + lg, sent)
+                started.extend(sent)
             else:
-                acc = own
-        for o in range(1, nz):
-            remote(rss.at[l, o], rsr.at[l, o], rs_s.at[l, o], rs_r.at[l, o], facing).wait_recv()
-            acc = acc + rsr[l, o].astype(F32)
-        fresh_x = (xs[l, me].astype(F32) + acc).astype(BF16)
-        if l + 1 < layers:
-            xs[l + 1, me] = fresh_x
-            sent = gather_start(xs.at[l + 1], 2 * l + 1)
-            gather_finish(xs.at[l + 1], 2 * l + 1, sent)
-            started += sent
-        else:
-            y_ref[...] = fresh_x
+                y_ref[pl.ds(g * rows, rows), :] = fresh_x
+
+    chains = [chain(g) for g in range(groups)]
+    live = list(range(groups))
+    step = 0
+    while live:
+        for g in list(live):
+            if step >= lag * g and next(chains[g], live) is live:
+                live.remove(g)
+        step += 1
     for copy in started:
         copy.wait_send()
 
@@ -466,22 +504,25 @@
     share = width // n
     fits = (
         cols == 128 and head_dim == 256 and he == 128 and heads == 8 and e_dim == 16
-        and share % 128 == 0 and n % 4 == 0 and rows == 128 and 8 % tok == 0
+        and share % 128 == 0 and n % 4 == 0 and n & (n - 1) == 0 and rows == 128 and 8 % tok == 0
     )
     if not fits:
         return plain_local(
             stream_in, state_in, norm_gain, query_weight, key_weight,
             value_weight, gate_weight, group_gain, output_weight,
         )
+    groups = 1
     nc = n // 2
-    be = seqs * e_dim
+    part = rows // groups
+    be = seqs * e_dim // groups
+    steps = layers * groups
     hbm = pl.BlockSpec(memory_space=pl.ANY)
     vmem = pl.BlockSpec(memory_space=pltpu.VMEM)
     dma = pltpu.SemaphoreType.DMA
     tables = jnp.asarray(rotary_tables(heads, tok, head_dim))
     flat = lambda w: jnp.transpose(w, (0, 2, 3, 1)).reshape(layers, he, width)
     y, new_state = pl.pallas_call(
-        functools.partial(kernel, n, head_dim),
+        functools.partial(kernel, n, head_dim, groups, LAG),
         name="retention",
         out_shape=(
             jax.ShapeDtypeStruct((rows, share), BF16),
@@ -490,35 +531,35 @@
         in_specs=[hbm, hbm, vmem, hbm, hbm, hbm, hbm, vmem, hbm, vmem],
         out_specs=(vmem, vmem),
         scratch_shapes=[
-            pltpu.VMEM((layers, n, rows, share), BF16),
-            pltpu.VMEM((rows, width), BF16),
+            pltpu.VMEM((steps, n, part, share), BF16),
+            pltpu.VMEM((groups, part, width), BF16),
             pltpu.VMEM((layers, width, 2 * cols), BF16),
             pltpu.VMEM((layers, 2 * he, width), BF16),
             pltpu.VMEM((layers, he, width), BF16),
-            pltpu.VMEM((layers, n, rows, 2 * cols), BF16),
-            pltpu.VMEM((heads, rows, head_dim), BF16),
-            pltpu.VMEM((he, rows), BF16),
-            pltpu.VMEM((layers, n, 2 * heads, rows), F32),
-            pltpu.VMEM((layers, nc, rows, share), BF16),
-            pltpu.VMEM((layers, nc, rows, share), BF16),
-            pltpu.VMEM((layers, nc // 2, rows, share), BF16),
-            pltpu.VMEM((layers, nc // 2, rows, share), BF16),
-            pltpu.VMEM((layers, nc // 2, rows, share), BF16),
-            pltpu.VMEM((layers, nc // 2, rows, share), BF16),
-            pltpu.VMEM((rows, be), BF16),
-            pltpu.VMEM((be, rows), BF16),
+            pltpu.VMEM((steps, n, part, 2 * cols), BF16),
+            pltpu.VMEM((groups * heads, part, head_dim), BF16),
+            pltpu.VMEM((groups, he, part), BF16),
+            pltpu.VMEM((steps, n, heads, 2 * part), F32),
+            pltpu.VMEM((steps, nc, part, share), BF16),
+            pltpu.VMEM((steps, nc, part, share), BF16),
+            pltpu.VMEM((steps, nc // 2, part, share), BF16),
+            pltpu.VMEM((steps, nc // 2, part, share), BF16),
+            pltpu.VMEM((steps, nc // 2, part, share), BF16),
+            pltpu.VMEM((steps, nc // 2, part, share), BF16),
+            pltpu.VMEM((part, be), BF16),
+            pltpu.VMEM((be, part), BF16),
             pltpu.VMEM((be, he), BF16),
-            dma((n + 6 * layers,)),
-            dma((2 * layers, n)),
-            dma((2 * layers, n)),
-            dma((layers, n)),
-            dma((layers, n)),
-            dma((layers, nc)),
-            dma((layers, nc)),
-            dma((layers, nc // 2)),
-            dma((layers, nc // 2)),
-            dma((layers, nc // 2)),
-            dma((layers, nc // 2)),
+            dma((groups * n + 6 * layers,)),
+            dma((2 * steps, n)),
+            dma((2 * steps, n)),
+            dma((steps, n)),
+            dma((steps, n)),
+            dma((steps, nc)),
+            dma((steps, nc)),
+            dma((steps, nc // 2)),
+            dma((steps, nc // 2)),
+            dma((steps, nc // 2)),
+            dma((steps, nc // 2)),
         ],
         compiler_params=pltpu.CompilerParams(
             collective_id=0, has_side_effects=True, vmem_limit_bytes=44 * 2**20

time: 95.3 us -> 92.1 us (0.966)
  Pallas kernels: 92.4 us -> 89.2 us
    pallas_call x1, Pallas kernels: 88.9 us -> 85.8 us  [local(): pl.pallas_call(functools.partial(kernel, n, head_dim, groups, LAG), name=...]
where the time goes in v3:
time: 92.1 us; the launch traced here: 91.9 us
  Pallas kernels  89.2 us (97%)
  local copies, waits for them, and re-layouts  2.06 us (2%)
    pallas_call x1, Pallas kernels, local(): pl.pallas_call(functools.partial(kernel, n, head_dim, groups, LAG), name=...  85.8 us
    pallas_call x1, Pallas kernels, local(): pl.pallas_call(store_kernel, name='store', out_shape=(jax.ShapeDtypeStruc...  3.41 us

profile of v3, /device:TPU:0, one launch (start us, length us, event | category | flops | bytes accessed | tf_op | source)
XLA Modules:
  0.0 91.9 jit_solution(18214433493446871272)
XLA Ops:
  0.6 0.0 copy-start
  0.6 0.0 copy-start.2
  0.7 0.0 copy-start.1
  0.7 1.4 %reshape.19.x_hbm = bf16[128,4096]{1,0:T(8,128)(2,1)S(1)} reshape(bf16[32,4,4096]{2,1,0:T(4,128)(2,1)} %param.10) | data formatting | bytes 2097152 | tf_op jit(solution)/shard_map/reshape | solution.py:568
  2.1 0.0 copy-done
  2.1 0.0 copy-done.2
  2.1 0.0 copy-done.1
  2.1 85.8 %retention.1 = (bf16[128,256]{1,0:T(8,128)(2,1)S(1)}, f32[2,32,8,16,256]{4,3,2,1,0:T(8,128)S(1)}) custom-call(bf16[128,4096]{1,0:T(8,128)(2,1)S(1)} %reshape.19.x_hbm, f32[2,32,8,16,256]{4,3,2,1,0:T(8,128)} %st_hbm.1, bf16[2,4096]{1,0:T(2,128)(2,1)S(1)} %copy-done.1, bf16[2,4096,128]{2,1,0:T(8,128)(2,1)} %qw_hbm.1, bf16[2,4096,128]{2,1,0:T(8,128)(2,1)} %kw_hbm.1, ...), custom_call_target="tpu_custom_call" | custom-call | tf_op jit(solution)/shard_map/retention/pallas_call | solution.py:524
  87.9 3.4 %store.1 = (bf16[128,256]{1,0:T(8,128)(2,1)S(1)}, f32[2,32,8,16,256]{4,3,2,1,0:T(8,128)}) custom-call(bf16[128,256]{1,0:T(8,128)(2,1)S(1)} %get-tuple-element.6.y_ref, f32[2,32,8,16,256]{4,3,2,1,0:T(8,128)S(1)} %get-tuple-element.7.state_ref), custom_call_target="tpu_custom_call" | custom-call | tf_op jit(solution)/shard_map/store/pallas_call | solution.py:572
  91.3 0.7 reshape.23
Async XLA Ops:
  0.6 1.4 %copy-start = (f32[5,8,8,128]{3,2,1,0:T(8,128)S(1)}, f32[5,8,8,128]{3,2,1,0:T(8,128)}, u32[]{:S(2)}) copy-start(f32[5,8,8,128]{3,2,1,0:T(8,128)} %constant.2.clone.tab_ref) | copy-start | bytes 491524
  0.6 1.4 %copy-start.2 = (bf16[2,8,16]{2,1,0:T(8,128)(2,1)S(1)}, bf16[2,8,16]{2,1,0:T(8,128)(2,1)}, u32[]{:S(2)}) copy-start(bf16[2,8,16]{2,1,0:T(8,128)(2,1)} %gg_ref.1) | copy-start | bytes 1540
  0.7 1.4 %copy-start.1 = (bf16[2,4096]{1,0:T(2,128)(2,1)S(1)}, bf16[2,4096]{1,0:T(2,128)(2,1)}, u32[]{:S(2)}) copy-start(bf16[2,4096]{1,0:T(2,128)(2,1)} %ng_ref.1) | copy-start | bytes 49156
